TPU v7x, 32 devices: a whole 2x2x4 slice. The times are simulated.
32 devices in a mesh: ep: 16 (over z, y, core), tp: 2 (over x).
Axes of the slice: x: 2, y: 2, z: 4, core: 2. Of those that a mesh axis runs over, the one named last changes fastest.
Arguments:
- tokens: bfloat16 [256, 2048], P('ep'), may hold values from -6 to 6
- positions: int32 [256], P('ep'), may hold values from 1024 to 16383
- state: float32 [256, 4, 128, 128], P('ep', 'tp'), may hold values from -1 to 1
- mix_gain: float32 [2048], replicated, may hold values from 0.1 to 1.9
- w_query: bfloat16 [2048, 512], P(None, 'tp'), may hold values from -0.125 to 0.125
- w_key: bfloat16 [2048, 512], P(None, 'tp'), may hold values from -0.125 to 0.125
- w_value: bfloat16 [2048, 512], P(None, 'tp'), may hold values from -0.125 to 0.125
- w_out: bfloat16 [512, 2048], P('tp'), may hold values from -0.25 to 0.25
- ffn_gain: float32 [2048], replicated, may hold values from 0.1 to 1.9
- branch_gate: bfloat16 [2048], replicated, may hold values from -0.125 to 0.125
- dense_gate: bfloat16 [2048, 4096], P('tp', 'ep'), may hold values from -0.125 to 0.125
- dense_up: bfloat16 [2048, 4096], P('tp', 'ep'), may hold values from -0.125 to 0.125
- dense_down: bfloat16 [4096, 2048], P('ep', 'tp'), may hold values from -0.09375 to 0.09375
- routes: int32 [256, 6], P('ep'), may hold values from 0 to 15, all different within a row; in each aligned block of 16 rows (0 to 15, 16 to 31, ...) at most 12 rows name the same one
- route_scores: float32 [256, 6], P('ep'), may hold values from 0.05 to 1
- expert_gate: bfloat16 [16, 2048, 512], P('ep', None, 'tp'), may hold values from -0.125 to 0.125
- expert_up: bfloat16 [16, 2048, 512], P('ep', None, 'tp'), may hold values from -0.125 to 0.125
- expert_down: bfloat16 [16, 512, 2048], P('ep', 'tp'), may hold values from -0.25 to 0.25
Outputs:
- layer_out: bfloat16 [256, 2048], P('ep', 'tp')
Inputs may be any that keep to these rules, and one draw needn't show every extreme that they name: `routes`: each row names 6 different experts. In each aligned block of 16 rows (the rows of one index of ep) no expert is named by more than 12 rows, a bound that some block reaches.
All inputs are finite; a program needn't handle non-finite values.
Results may differ from a plain program's by a relative error of at most 0.012.
Values may be sent and summed in bfloat16 or wider, within the bound.
A program may use at most 64 MiB of HBM per device.

v0:
```python
import jax
import jax.numpy as jnp
from jax import lax
from jax.sharding import PartitionSpec as P

EPS = 1e-06


def normalize(inputs, scale_vec):
    values = inputs.astype(jnp.float32)
    return values * lax.rsqrt(jnp.mean(values * values, axis=-1, keepdims=True) + EPS) * scale_vec


def rotate(vectors, where):
    half = vectors.shape[-1] // 2
    inverse = 1.0 / 10000.0 ** jnp.linspace(0.0, 1.0, half, dtype=jnp.float32)
    angle = where.astype(jnp.float32)[:, None] * inverse[None, :]
    cosine = jnp.cos(angle)[:, None, :]
    sine = jnp.sin(angle)[:, None, :]
    first = vectors[..., :half]
    second = vectors[..., half:]
    return jnp.concatenate(
        [first * cosine - second * sine, second * cosine + first * sine], axis=-1
    )


def on_device(
    tokens,
    positions,
    state,
    mix_gain,
    w_query,
    w_key,
    w_value,
    w_out,
    ffn_gain,
    branch_gate,
    dense_gate,
    dense_up,
    dense_down,
    routes,
    route_scores,
    expert_gate,
    expert_up,
    expert_down,
):
    sequences = tokens.shape[0]
    model_width = tokens.shape[1]
    tp_count = lax.axis_size("tp")
    ep_count = lax.axis_size("ep")
    columns = model_width // tp_count
    tp_index = lax.axis_index("tp")
    local_heads = state.shape[1]
    head_dim = state.shape[2]
    normed = normalize(tokens, mix_gain).astype(jnp.bfloat16)
    query_vec = jnp.dot(normed, w_query, preferred_element_type=jnp.float32).reshape(
        sequences, local_heads, head_dim
    )
    key_vec = jnp.dot(normed, w_key, preferred_element_type=jnp.float32).reshape(
        sequences, local_heads, head_dim
    )
    value_vec = jnp.dot(normed, w_value, preferred_element_type=jnp.float32).reshape(
        sequences, local_heads, head_dim
    )
    query_vec = rotate(query_vec, positions)
    key_vec = rotate(key_vec, positions) * head_dim ** (-0.5)
    all_heads = local_heads * tp_count
    head_index = (tp_index * local_heads + jnp.arange(local_heads, dtype=jnp.int32)).astype(
        jnp.float32
    )
    decay_rate = 1.0 - 2.0 ** (-5.0 - 5.0 * head_index / (all_heads - 1))
    new_state = (
        decay_rate[None, :, None, None] * state + key_vec[:, :, :, None] * value_vec[:, :, None, :]
    )
    retrieved = jnp.einsum("bhd,bhde->bhe", query_vec, new_state, precision=lax.Precision.HIGHEST)
    retrieved = retrieved * lax.rsqrt(jnp.mean(retrieved * retrieved, axis=-1, keepdims=True) + EPS)
    retrieved = retrieved.reshape(sequences, local_heads * head_dim).astype(jnp.bfloat16)
    head_partial = jnp.dot(retrieved, w_out, preferred_element_type=jnp.float32).astype(
        jnp.bfloat16
    )
    mixer_out = lax.psum(head_partial.astype(jnp.float32).astype(jnp.bfloat16), "tp").astype(
        jnp.float32
    )
    after_mix = tokens.astype(jnp.float32) + mixer_out
    ffn_in = normalize(after_mix, ffn_gain).astype(jnp.bfloat16)
    own_cols = lax.dynamic_slice_in_dim(ffn_in, tp_index * columns, columns, 1)
    per_device = expert_gate.shape[0]
    experts = per_device * ep_count
    fanout = routes.shape[1]
    capacity = max(2, min(sequences, 2 * sequences * fanout // experts))
    slot_count = experts * capacity
    marks = (routes[:, :, None] == jnp.arange(experts, dtype=jnp.int32)[None, None, :]).astype(
        jnp.int32
    )
    flattened = marks.reshape(sequences * fanout, experts)
    ranking = jnp.sum((jnp.cumsum(flattened, axis=0) - flattened) * flattened, axis=1).reshape(
        sequences, fanout
    )
    slot_index = routes * capacity + ranking
    matches = jnp.arange(slot_count, dtype=jnp.int32)[:, None, None] == slot_index[None]
    placing = jnp.any(matches, axis=2).astype(jnp.bfloat16)
    route_weights = route_scores / jnp.sum(route_scores, axis=1, keepdims=True)
    combining = jnp.sum(jnp.where(matches, route_weights[None], 0.0), axis=2).T
    packed = jnp.dot(placing, own_cols, preferred_element_type=jnp.float32).astype(jnp.bfloat16)
    packed = packed.reshape(experts, capacity, own_cols.shape[1])
    received = lax.all_to_all(packed, "ep", split_axis=0, concat_axis=0, tiled=True)
    received = lax.all_gather(received, "tp", axis=2, tiled=True)
    count = received.shape[1]
    grouped = received.reshape(ep_count, per_device, count, model_width)
    gate_pre = jnp.einsum(
        "skcd,kdw->skcw", grouped, expert_gate, preferred_element_type=jnp.float32
    )
    up_pre = jnp.einsum("skcd,kdw->skcw", grouped, expert_up, preferred_element_type=jnp.float32)
    hidden = (jax.nn.silu(gate_pre) * up_pre).astype(jnp.bfloat16)
    partial_out = jnp.einsum(
        "skcw,kwd->skcd", hidden, expert_down, preferred_element_type=jnp.float32
    )
    blocks_out = partial_out.astype(jnp.bfloat16).reshape(
        ep_count, per_device, count, tp_count, columns
    )
    traded = lax.all_to_all(blocks_out, "tp", split_axis=3, concat_axis=3, tiled=True)
    mine = jnp.sum(traded.astype(jnp.float32), axis=3).astype(jnp.bfloat16)
    mine = mine.reshape(ep_count * per_device, count, columns)
    returned = lax.all_to_all(mine, "ep", split_axis=0, concat_axis=0, tiled=True)
    experts_out = jnp.dot(
        combining,
        returned.reshape(slot_count, columns).astype(jnp.float32),
        precision=lax.Precision.HIGHEST,
    )
    hidden_units = dense_gate.shape[1]
    both_weights = jnp.concatenate([dense_gate, dense_up], axis=1)
    pre_parts = jnp.dot(
        lax.all_gather(own_cols, "ep", axis=0, tiled=True),
        both_weights,
        preferred_element_type=jnp.float32,
    ).astype(jnp.bfloat16)
    pre_total = lax.psum(pre_parts.astype(jnp.float32).astype(jnp.bfloat16), "tp").astype(
        jnp.float32
    )
    dense_hidden = (jax.nn.silu(pre_total[:, :hidden_units]) * pre_total[:, hidden_units:]).astype(
        jnp.bfloat16
    )
    dense_out = lax.psum_scatter(
        jnp.dot(dense_hidden, dense_down, preferred_element_type=jnp.float32),
        "ep",
        scatter_dimension=0,
        tiled=True,
    )
    branch_weight = jax.nn.sigmoid(jnp.dot(ffn_in, branch_gate, preferred_element_type=jnp.float32))
    residual_cols = lax.dynamic_slice_in_dim(after_mix, tp_index * columns, columns, 1)
    layer_out = residual_cols + experts_out + branch_weight[:, None] * dense_out
    return layer_out.astype(jnp.bfloat16)


def solution(mesh):
    placed = (
        P("ep", None),
        P("ep"),
        P("ep", "tp", None, None),
        P(),
        P(None, "tp"),
        P(None, "tp"),
        P(None, "tp"),
        P("tp", None),
        P(),
        P(),
        P("tp", "ep"),
        P("tp", "ep"),
        P("ep", "tp"),
        P("ep", None),
        P("ep", None),
        P("ep", None, "tp"),
        P("ep", None, "tp"),
        P("ep", "tp", None),
    )
    return jax.shard_map(
        on_device, mesh=mesh, in_specs=placed, out_specs=P("ep", "tp"), check_vma=False
    )
```

profile of v0, /device:TPU:0, one launch (start us, length us, event | category | flops | bytes accessed | tf_op | source)
XLA Modules:
  0.0 169.2 jit_solution(17816289287856958037)
XLA Ops:
  6.6 0.8 convert_element_type.77
  7.4 1.0 fusion.30
  8.5 1.6 fusion.47
  10.1 1.6 fusion.45
  11.7 1.5 fusion.49
  13.2 0.1 fusion.41
  13.3 0.1 multiply_cosine_fusion
  13.4 0.1 multiply_subtract_fusion
  13.5 0.1 pad_maximum_fusion
  13.7 2.1 %fusion = f32[16,2,1,128]{3,2,1,0:T(1,128)S(1)} fusion(f32[16,2,128,1]{2,3,1,0:T(1,128)S(1)} %bitcast.86, f32[16,2,128,128]{3,2,1,0:T(8,128)S(1)} %copy-done.2, f32[16,2,128]{2,1,0:T(2,128)S(1)} %mul.244, f32[16,2,128]{2,1,0:T(2,128)S(1)} %get-tuple-element.17, f32[2]{0:T(128)S(1)} %power_subtract_fusion), kind=kOutput, calls=%fused_computation.2 | convolution fusion | flops 7864320 | bytes 2162696 | tf_op jit(solution)/shard_map/bhd,bhde->bhe/dot_general | solution.py:75
  15.7 0.1 multiply_reduce_fusion.1
  15.8 0.1 multiply_convert_fusion.1
  15.9 0.9 convolution_convert_fusion.1
  16.9 0.1 copy.59
  16.9 0.1 eq.30
  17.0 0.1 fusion.38
  17.1 0.1 reduce_window_sum.11
  17.3 0.2 select_reduce_fusion.1
  17.4 0.1 reshape.154
  17.5 0.1 copy.60
  17.6 0.1 fusion.37
  17.7 23.0 %all-reduce.3.cloned.1.call-done = bf16[16,2048]{1,0:T(8,128)(2,1)} async-done(((bf16[16,2048]{1,0:T(8,128)(2,1)}), bf16[16,2048]{1,0:T(8,128)(2,1)}) %all-reduce.3.cloned.1.call-update) | async-done | bytes 65552 | tf_op jit(solution)/shard_map/psum | solution.py:81
  40.7 1.6 convert_add_fusion
  42.3 0.9 multiply_convert_fusion
  43.3 22.9 %all_gather.7 = bf16[256,1024]{1,0:T(8,128)(2,1)S(1)} all-gather(bf16[16,1024]{1,0:T(8,128)(2,1)S(1)} %constant_dynamic-slice_fusion), channel_id=1, replica_groups=mesh['ep'=16,'tp'=2] {'ep'}, dimensions={0}, use_global_device_ids=true | all-gather | bytes 557056 | tf_op jit(solution)/shard_map/all_gather | solution.py:133
  66.2 0.3 convolution_convert_fusion.2
  66.5 0.9 reshape.155
  67.4 3.6 %all-to-all-start = ((bf16[16,12,1024]{2,1,0:T(8,128)(2,1)}), bf16[16,12,1024]{2,1,0:T(8,128)(2,1)S(1)}, u32[]{:S(2)}, u32[]{:S(2)}) async-start(bf16[16,12,1024]{2,1,0:T(8,128)(2,1)} %reshape.155), calls=%async_computation | async-start | bytes 1048576 | tf_op jit(solution)/shard_map/all_to_all | solution.py:106
  71.0 0.0 all-reduce.5.cloned.1.call-start
  71.0 2.2 %convolution_convert_fusion.3 = bf16[256,512]{1,0:T(8,128)(2,1)} fusion(bf16[256,1024]{1,0:T(8,128)(2,1)S(1)} %all_gather.7, bf16[1024,256]{1,0:T(8,128)(2,1)S(1)} %copy-done.12, bf16[1024,256]{1,0:T(8,128)(2,1)} %param.30), kind=kOutput, calls=%fused_computation.7 | convolution fusion | flops 270663680 | bytes 1835008 | tf_op jit(solution)/shard_map/dot_general | solution.py:132
  73.3 24.4 %all-reduce.5.cloned.1.call-done = bf16[256,512]{1,0:T(8,128)(2,1)} async-done(((bf16[256,512]{1,0:T(8,128)(2,1)}), bf16[256,512]{1,0:T(8,128)(2,1)}) %all-reduce.5.cloned.1.call-update) | async-done | bytes 262160 | tf_op jit(solution)/shard_map/psum | solution.py:137
  97.7 1.0 convert_element_type.92
  98.8 1.3 fusion.33
  100.1 0.2 copy.61
  100.3 11.0 %all_gather.6 = bf16[16,12,2048]{2,0,1:T(8,128)(2,1)S(1)} all-gather(bf16[16,12,1024]{2,0,1:T(8,128)(2,1)S(1)} %copy.61), channel_id=1, replica_groups=mesh['ep'=16,'tp'=2] {'tp'}, dimensions={2}, use_global_device_ids=true | all-gather | bytes 1179648 | tf_op jit(solution)/shard_map/all_gather | solution.py:107
  111.4 1.1 convolution_bitcast_fusion.1
  112.4 2.3 %convolution_convert_fusion = bf16[16,12,2048]{2,0,1:T(8,128)(2,1)S(1)} fusion(bf16[1,256,2048]{2,1,0:T(8,128)(2,1)S(1)} %copy-done, bf16[16,12,2048]{2,0,1:T(8,128)(2,1)S(1)} %all_gather.6, bf16[1,2048,256]{2,1,0:T(8,128)(2,1)} %param.36, f32[16,1,12,256]{3,0,2,1:T(8,128)} %convolution_bitcast_fusion.1), kind=kOutput, calls=%fused_computation | convolution fusion | flops 403341312 | bytes 3866624 | tf_op jit(solution)/shard_map/skcw,kwd->skcd/dot_general | solution.py:115
  114.7 0.1 copy.77
  114.8 12.1 %all_to_all.15 = bf16[16,1,12,2,1024]{4,0,2,1,3:T(8,128)(2,1)S(1)} all-to-all(bf16[16,1,12,2,1024]{4,0,2,1,3:T(8,128)(2,1)S(1)} %bitcast.82), channel_id=1, replica_groups=mesh['ep'=16,'tp'=2] {'tp'}, dimensions={3} | all-to-all | bytes 1572864 | tf_op jit(solution)/shard_map/all_to_all | solution.py:121
  126.9 0.2 reduce_sum.72
  127.1 1.0 copy.64
  128.2 5.6 %all-to-all-start.2 = ((bf16[16,12,1024]{2,1,0:T(8,128)(2,1)}), bf16[16,12,1024]{2,1,0:T(8,128)(2,1)S(1)}, u32[]{:S(2)}, u32[]{:S(2)}) async-start(bf16[16,12,1024]{2,1,0:T(8,128)(2,1)} %copy.64), calls=%async_computation.2 | async-start | bytes 1048576 | tf_op jit(solution)/shard_map/all_to_all | solution.py:124
  133.9 0.1 select_reduce_fusion
  134.0 0.1 fusion.12
  134.1 14.8 %all-to-all-done.2 = bf16[16,12,1024]{2,1,0:T(8,128)(2,1)S(1)} async-done(((bf16[16,12,1024]{2,1,0:T(8,128)(2,1)}), bf16[16,12,1024]{2,1,0:T(8,128)(2,1)S(1)}, u32[]{:S(2)}, u32[]{:S(2)}) %all-to-all-start.2) | async-done | bytes 393248 | tf_op jit(solution)/shard_map/all_to_all | solution.py:124
  148.9 0.1 reshape.161
  149.0 11.9 %reduce-scatter.2.cloned.1.call-done = f32[16,1024]{1,0:T(8,128)} async-done(((f32[256,1024]{1,0:T(8,128)}), f32[16,1024]{1,0:T(8,128)}) %reduce-scatter.2.cloned.1.call-update) | async-done | bytes 65552 | tf_op jit(solution)/shard_map/reduce_scatter | solution.py:143
  160.9 1.7 %fusion.8 = bf16[16,1024]{1,0:T(8,128)(2,1)} fusion(f32[192,16]{0,1:T(8,128)S(1)} %select_reduce_fusion, bf16[192,1024]{1,0:T(8,128)(2,1)S(1)} %reshape.161, f32[16,1024]{1,0:T(8,128)} %reduce-scatter.2.cloned.1.call-done, f32[16,2048]{1,0:T(8,128)S(1)} %copy-done.6, s32[]{:T(128)S(6)} %select_n.8, f32[16]{0:T(128)S(1)} %fusion.12), kind=kOutput, calls=%fused_computation.15 | convolution fusion | flops 37814272 | bytes 569412 | tf_op jit(solution)/shard_map/dot_general | solution.py:125
  (45 shorter events, 0.3 us)
Async XLA Ops:
  6.5 105.9 %copy-start = (bf16[1,256,2048]{2,1,0:T(8,128)(2,1)S(1)}, bf16[1,256,2048]{2,1,0:T(8,128)(2,1)}, u32[]{:S(2)}) copy-start(bf16[1,256,2048]{2,1,0:T(8,128)(2,1)} %param.37) | copy-start | bytes 3145732
  6.5 5.1 %copy-start.1 = (bf16[16,2048]{1,0:T(8,128)(2,1)S(1)}, bf16[16,2048]{1,0:T(8,128)(2,1)}, u32[]{:S(2)}) copy-start(bf16[16,2048]{1,0:T(8,128)(2,1)} %param.20) | copy-start | bytes 196612
  6.5 5.1 %copy-start.7 = (f32[2048]{0:T(1024)S(1)}, f32[2048]{0:T(1024)}, u32[]{:S(2)}) copy-start(f32[2048]{0:T(1024)} %param.23) | copy-start | bytes 24580
  6.5 7.1 %copy-start.2 = (f32[16,2,128,128]{3,2,1,0:T(8,128)S(1)}, f32[16,2,128,128]{3,2,1,0:T(8,128)}, u32[]{:S(2)}) copy-start(f32[16,2,128,128]{3,2,1,0:T(8,128)} %param.22) | copy-start | bytes 6291460
  6.5 34.1 %all-reduce.3.cloned.1.call-start = ((), (), s32[]{:S(2)}) async-start(), calls=%async_computation.4 | async-start | bytes 131072 | tf_op jit(solution)/shard_map/psum | solution.py:81
  13.2 3.7 %copy-start.8 = (s32[16,6]{0,1:T(8,128)S(1)}, s32[16,6]{0,1:T(8,128)}, u32[]{:S(2)}) copy-start(s32[16,6]{0,1:T(8,128)} %param.33) | copy-start | bytes 1156
  13.2 2.7 %copy-start.3 = (bf16[256,2048]{1,0:T(8,128)(2,1)S(1)}, bf16[256,2048]{1,0:T(8,128)(2,1)}, u32[]{:S(2)}) copy-start(bf16[256,2048]{1,0:T(8,128)(2,1)} %param.27) | copy-start | bytes 3145732
  13.4 28.9 %copy-start.10 = (f32[2048]{0:T(1024)S(1)}, f32[2048]{0:T(1024)}, u32[]{:S(2)}) copy-start(f32[2048]{0:T(1024)} %param.28) | copy-start | bytes 24580
  16.8 54.2 %copy-start.12 = (bf16[1024,256]{1,0:T(8,128)(2,1)S(1)}, bf16[1024,256]{1,0:T(8,128)(2,1)}, u32[]{:S(2)}) copy-start(bf16[1024,256]{1,0:T(8,128)(2,1)} %param.31) | copy-start | bytes 1572868
  67.4 32.7 %all-to-all-start = ((bf16[16,12,1024]{2,1,0:T(8,128)(2,1)}), bf16[16,12,1024]{2,1,0:T(8,128)(2,1)S(1)}, u32[]{:S(2)}, u32[]{:S(2)}) async-start(bf16[16,12,1024]{2,1,0:T(8,128)(2,1)} %reshape.155), calls=%async_computation | async-start | bytes 1048576 | tf_op jit(solution)/shard_map/all_to_all | solution.py:106
  70.9 27.8 %copy-start.5 = (bf16[256,1024]{1,0:T(8,128)(2,1)S(1)}, bf16[256,1024]{1,0:T(8,128)(2,1)}, u32[]{:S(2)}) copy-start(bf16[256,1024]{1,0:T(8,128)(2,1)} %param.32) | copy-start | bytes 1572868
  71.0 26.8 %all-reduce.5.cloned.1.call-start = ((), (), s32[]{:S(2)}) async-start(), calls=%async_computation.5 | async-start | bytes 524288 | tf_op jit(solution)/shard_map/psum | solution.py:137
  73.3 87.6 %reduce-scatter.2.cloned.1.call-start = ((), (), s32[]{:S(2)}) async-start(), calls=%async_computation.6 | async-start | bytes 1114112 | tf_op jit(solution)/shard_map/reduce_scatter | solution.py:143
  98.8 12.6 %copy-start.4 = (bf16[1,2048,256]{2,1,0:T(8,128)(2,1)S(1)}, bf16[1,2048,256]{2,1,0:T(8,128)(2,1)}, u32[]{:S(2)}) copy-start(bf16[1,2048,256]{2,1,0:T(8,128)(2,1)} %param.35) | copy-start | bytes 3145732
  114.8 19.0 %copy-start.11 = (bf16[2048]{0:T(1024)(128)(2,1)S(1)}, bf16[2048]{0:T(1024)(128)(2,1)}, u32[]{:S(2)}) copy-start(bf16[2048]{0:T(1024)(128)(2,1)} %param.29) | copy-start | bytes 12292
  114.8 19.0 %copy-start.9 = (f32[16,6]{0,1:T(8,128)S(1)}, f32[16,6]{0,1:T(8,128)}, u32[]{:S(2)}) copy-start(f32[16,6]{0,1:T(8,128)} %param.34) | copy-start | bytes 1156
  126.9 34.0 %copy-start.6 = (f32[16,2048]{1,0:T(8,128)S(1)}, f32[16,2048]{1,0:T(8,128)}, u32[]{:S(2)}) copy-start(f32[16,2048]{1,0:T(8,128)} %get-tuple-element.6) | copy-start | bytes 393220
  128.2 20.7 %all-to-all-start.2 = ((bf16[16,12,1024]{2,1,0:T(8,128)(2,1)}), bf16[16,12,1024]{2,1,0:T(8,128)(2,1)S(1)}, u32[]{:S(2)}, u32[]{:S(2)}) async-start(bf16[16,12,1024]{2,1,0:T(8,128)(2,1)} %copy.64), calls=%async_computation.2 | async-start | bytes 1048576 | tf_op jit(solution)/shard_map/all_to_all | solution.py:124
Sparse Core Ops, SparseCore 0:
  17.0 23.6 all-reduce.2
  74.0 23.6 all-reduce.4
  101.4 59.4 reduce-scatter.1
where the time goes:
time: 170 us; the launch traced here: 169 us
  waiting for transfers between devices  74.1 us (44%)
  blocking collectives  46 us (27%)
  matrix products  16.6 us (10%)
  between operations  13.5 us (8%)
  starting transfers between devices  9.31 us (5%)
  other arithmetic  6.78 us (4%)
  local copies, waits for them, and re-layouts  2.79 us (2%)
    psum x1, waiting for transfers between devices, on_device(): lax.psum(pre_parts.astype(jnp.float32).astype(jnp.bfloat16), 'tp')  24.4 us
    psum x1, waiting for transfers between devices, on_device(): lax.psum(head_partial.astype(jnp.float32).astype(jnp.bfloat16), 'tp')  23 us
    all_gather x1, blocking collectives, on_device(): lax.all_gather(own_cols, 'ep', axis=0, tiled=True)  22.9 us
    all_to_all x1, waiting for transfers between devices, on_device(): lax.all_to_all(mine, 'ep', split_axis=0, concat_axis=0, tiled=True)  14.8 us
    all_to_all x1, blocking collectives, on_device(): lax.all_to_all(blocks_out, 'tp', split_axis=3, concat_axis=3, tiled=True)  12.1 us
    reduce_scatter x1, waiting for transfers between devices, on_device(): lax.psum_scatter(jnp.dot(dense_hidden, dense_down, preferred_element_type...  11.9 us
    all_gather x1, blocking collectives, on_device(): received = lax.all_gather(received, 'tp', axis=2, tiled=True)  11 us
    all_to_all x1, starting transfers between devices, on_device(): lax.all_to_all(mine, 'ep', split_axis=0, concat_axis=0, tiled=True)  5.62 us
  transfers between devices with their start and end apart: 5, of which 4 were waited for; matrix products, arithmetic and copies ran while one was open for 6% of the time, Pallas kernels for 0%

commit v1 on v0

--- a/solution.py
+++ b/solution.py
@@ -78,7 +78,8 @@
     head_partial = jnp.dot(retrieved, w_out, preferred_element_type=jnp.float32).astype(
         jnp.bfloat16
     )
-    mixer_out = lax.psum(head_partial.astype(jnp.float32).astype(jnp.bfloat16), "tp").astype(
+    apply_weights = lambda array_in: jnp.sum(lax.all_gather(array_in, axis_name="tp"), axis=0)
+    mixer_out = apply_weights(head_partial.astype(jnp.float32).astype(jnp.bfloat16)).astype(
         jnp.float32
     )
     after_mix = tokens.astype(jnp.float32) + mixer_out

time: 170 us -> 158 us (0.929)
  waiting for transfers between devices: 74.1 us -> 50.1 us
  blocking collectives: 46 us -> 56 us
  starting transfers between devices: 9.31 us -> 12.2 us
    psum x1 -> x0, waiting for transfers between devices: 23 us -> none  [on_device(): lax.psum(head_partial.astype(jnp.float32).astype(jnp.bfloat16), 'tp')]
    all_gather x0 -> x1, blocking collectives: none -> 5.99 us  [on_device(): lax.all_gather(array_in, axis_name='tp')]
    all_gather x1, blocking collectives: 22.9 us -> 26.8 us  [on_device(): lax.all_gather(own_cols, 'ep', axis=0, tiled=True)]
    all_to_all x1, starting transfers between devices: 3.57 us -> 6.48 us  [on_device(): lax.all_to_all(packed, 'ep', split_axis=0, concat_axis=0, tiled=True)]
    psum x1, waiting for transfers between devices: 24.4 us -> 21.8 us  [on_device(): lax.psum(pre_parts.astype(jnp.float32).astype(jnp.bfloat16), 'tp')]
  transfers between devices with their start and end apart: 5 -> 4, of which waited for: 4 -> 3; matrix products, arithmetic and copies ran while one was open for 6% -> 6% of each run, Pallas kernels for 0% -> 0%
where the time goes in v1:
time: 158 us; the launch traced here: 157 us
  blocking collectives  56 us (35%)
  waiting for transfers between devices  50.1 us (32%)
  matrix products  16.5 us (10%)
  between operations  13.7 us (9%)
  starting transfers between devices  12.2 us (8%)
  other arithmetic  5.13 us (3%)
  local copies, waits for them, and re-layouts  3.48 us (2%)
    all_gather x1, blocking collectives, on_device(): lax.all_gather(own_cols, 'ep', axis=0, tiled=True)  26.8 us
    psum x1, waiting for transfers between devices, on_device(): lax.psum(pre_parts.astype(jnp.float32).astype(jnp.bfloat16), 'tp')  21.8 us
    all_to_all x1, waiting for transfers between devices, on_device(): lax.all_to_all(mine, 'ep', split_axis=0, concat_axis=0, tiled=True)  15.2 us
    reduce_scatter x1, waiting for transfers between devices, on_device(): lax.psum_scatter(jnp.dot(dense_hidden, dense_down, preferred_element_type...  13 us
    all_to_all x1, blocking collectives, on_device(): lax.all_to_all(blocks_out, 'tp', split_axis=3, concat_axis=3, tiled=True)  12.1 us
    all_gather x1, blocking collectives, on_device(): received = lax.all_gather(received, 'tp', axis=2, tiled=True)  11 us
    all_to_all x1, starting transfers between devices, on_device(): lax.all_to_all(packed, 'ep', split_axis=0, concat_axis=0, tiled=True)  6.48 us
    all_gather x1, blocking collectives, on_device(): lax.all_gather(array_in, axis_name='tp')  5.99 us
  transfers between devices with their start and end apart: 4, of which 3 were waited for; matrix products, arithmetic and copies ran while one was open for 6% of the time, Pallas kernels for 0%

profile of v1, /device:TPU:0, one launch (start us, length us, event | category | flops | bytes accessed | tf_op | source)
XLA Modules:
  0.0 157.1 jit_solution(18438197014540999177)
XLA Ops:
  6.6 0.8 convert_element_type.79
  7.4 1.0 fusion.30
  8.4 0.8 copy.59
  9.2 0.1 eq.30
  9.3 1.6 fusion.47
  10.9 1.6 fusion.45
  12.5 1.5 fusion.49
  14.0 0.1 fusion.41
  14.1 0.1 multiply_cosine_fusion
  14.2 0.1 multiply_subtract_fusion
  14.3 0.1 pad_maximum_fusion
  14.5 2.1 %fusion = f32[16,2,1,128]{3,2,1,0:T(1,128)S(1)} fusion(f32[16,2,128,1]{2,3,1,0:T(1,128)S(1)} %bitcast.88, f32[16,2,128,128]{3,2,1,0:T(8,128)S(1)} %copy-done.2, f32[16,2,128]{2,1,0:T(2,128)S(1)} %mul.244, f32[16,2,128]{2,1,0:T(2,128)S(1)} %get-tuple-element.17, f32[2]{0:T(128)S(1)} %power_subtract_fusion), kind=kOutput, calls=%fused_computation.2 | convolution fusion | flops 7864320 | bytes 2162696 | tf_op jit(solution)/shard_map/bhd,bhde->bhe/dot_general | solution.py:75
  16.5 0.1 multiply_reduce_fusion.1
  16.7 0.1 multiply_convert_fusion.1
  16.7 0.1 fusion.38
  16.8 0.1 reduce_window_sum.11
  17.0 0.2 select_reduce_fusion.1
  17.1 0.1 reshape.154
  17.2 0.1 copy.60
  17.3 0.1 fusion.37
  17.4 1.5 convolution_convert_fusion.1
  18.9 6.0 %all-gather = bf16[32,2048]{1,0:T(8,128)(2,1)S(1)} all-gather(bf16[16,2048]{1,0:T(8,128)(2,1)S(1)} %convolution_convert_fusion.1), channel_id=2, replica_groups=mesh['ep'=16,'tp'=2] {'tp'}, dimensions={0}, use_global_device_ids=true | all-gather | bytes 196608 | tf_op jit(solution)/shard_map/all_gather | solution.py:81
  24.9 0.8 convert_add_fusion
  25.7 0.1 multiply_convert_fusion
  25.8 0.3 convolution_convert_fusion.2
  26.1 0.9 reshape.155
  27.0 6.5 %all-to-all-start = ((bf16[16,12,1024]{2,1,0:T(8,128)(2,1)}), bf16[16,12,1024]{2,1,0:T(8,128)(2,1)S(1)}, u32[]{:S(2)}, u32[]{:S(2)}) async-start(bf16[16,12,1024]{2,1,0:T(8,128)(2,1)} %reshape.155), calls=%async_computation | async-start | bytes 1048576 | tf_op jit(solution)/shard_map/all_to_all | solution.py:107
  33.5 0.0 all-reduce.2.cloned.1.call-start
  33.6 26.8 %all_gather.15 = bf16[256,1024]{1,0:T(8,128)(2,1)S(1)} all-gather(bf16[16,1024]{1,0:T(8,128)(2,1)S(1)} %constant_dynamic-slice_fusion), channel_id=1, replica_groups=mesh['ep'=16,'tp'=2] {'ep'}, dimensions={0}, use_global_device_ids=true | all-gather | bytes 557056 | tf_op jit(solution)/shard_map/all_gather | solution.py:134
  60.4 2.2 %convolution_convert_fusion.3 = bf16[256,512]{1,0:T(8,128)(2,1)} fusion(bf16[256,1024]{1,0:T(8,128)(2,1)S(1)} %all_gather.15, bf16[1024,256]{1,0:T(8,128)(2,1)S(1)} %copy-done.11, bf16[1024,256]{1,0:T(8,128)(2,1)} %param.30), kind=kOutput, calls=%fused_computation.7 | convolution fusion | flops 270663680 | bytes 1835008 | tf_op jit(solution)/shard_map/dot_general | solution.py:133
  62.7 21.8 %all-reduce.2.cloned.1.call-done = bf16[256,512]{1,0:T(8,128)(2,1)} async-done(((bf16[256,512]{1,0:T(8,128)(2,1)}), bf16[256,512]{1,0:T(8,128)(2,1)}) %all-reduce.2.cloned.1.call-update) | async-done | bytes 262160 | tf_op jit(solution)/shard_map/psum | solution.py:138
  84.5 1.0 convert_element_type.94
  85.5 1.3 fusion.33
  86.9 0.2 copy.61
  87.1 11.0 %all_gather.14 = bf16[16,12,2048]{2,0,1:T(8,128)(2,1)S(1)} all-gather(bf16[16,12,1024]{2,0,1:T(8,128)(2,1)S(1)} %copy.61), channel_id=1, replica_groups=mesh['ep'=16,'tp'=2] {'tp'}, dimensions={2}, use_global_device_ids=true | all-gather | bytes 1179648 | tf_op jit(solution)/shard_map/all_gather | solution.py:108
  98.1 0.4 convolution_bitcast_fusion.1
  98.5 2.3 %convolution_convert_fusion = bf16[16,12,2048]{2,0,1:T(8,128)(2,1)S(1)} fusion(bf16[1,256,2048]{2,1,0:T(8,128)(2,1)S(1)} %copy-done, bf16[16,12,2048]{2,0,1:T(8,128)(2,1)S(1)} %all_gather.14, bf16[1,2048,256]{2,1,0:T(8,128)(2,1)} %param.36, f32[16,1,12,256]{3,0,2,1:T(8,128)S(1)} %convolution_bitcast_fusion.1), kind=kOutput, calls=%fused_computation | convolution fusion | flops 403341312 | bytes 3866624 | tf_op jit(solution)/shard_map/skcw,kwd->skcd/dot_general | solution.py:116
  100.8 0.1 copy.77
  100.9 12.1 %all_to_all.15 = bf16[16,1,12,2,1024]{4,0,2,1,3:T(8,128)(2,1)S(1)} all-to-all(bf16[16,1,12,2,1024]{4,0,2,1,3:T(8,128)(2,1)S(1)} %bitcast.83), channel_id=1, replica_groups=mesh['ep'=16,'tp'=2] {'tp'}, dimensions={3} | all-to-all | bytes 1572864 | tf_op jit(solution)/shard_map/all_to_all | solution.py:122
  113.0 0.2 reduce_sum.85
  113.2 1.0 copy.64
  114.2 5.6 %all-to-all-start.2 = ((bf16[16,12,1024]{2,1,0:T(8,128)(2,1)}), bf16[16,12,1024]{2,1,0:T(8,128)(2,1)S(1)}, u32[]{:S(2)}, u32[]{:S(2)}) async-start(bf16[16,12,1024]{2,1,0:T(8,128)(2,1)} %copy.64), calls=%async_computation.2 | async-start | bytes 1048576 | tf_op jit(solution)/shard_map/all_to_all | solution.py:125
  119.9 0.1 select_reduce_fusion
  120.0 0.1 fusion.12
  120.2 15.2 %all-to-all-done.2 = bf16[16,12,1024]{2,1,0:T(8,128)(2,1)S(1)} async-done(((bf16[16,12,1024]{2,1,0:T(8,128)(2,1)}), bf16[16,12,1024]{2,1,0:T(8,128)(2,1)S(1)}, u32[]{:S(2)}, u32[]{:S(2)}) %all-to-all-start.2) | async-done | bytes 393248 | tf_op jit(solution)/shard_map/all_to_all | solution.py:125
  135.3 0.1 reshape.161
  135.4 13.0 %reduce-scatter.2.cloned.1.call-done = f32[16,1024]{1,0:T(8,128)} async-done(((f32[256,1024]{1,0:T(8,128)}), f32[16,1024]{1,0:T(8,128)}) %reduce-scatter.2.cloned.1.call-update) | async-done | bytes 65552 | tf_op jit(solution)/shard_map/reduce_scatter | solution.py:144
  148.5 1.7 %fusion.8 = bf16[16,1024]{1,0:T(8,128)(2,1)} fusion(f32[192,16]{0,1:T(8,128)S(1)} %select_reduce_fusion, bf16[192,1024]{1,0:T(8,128)(2,1)S(1)} %reshape.161, f32[16,1024]{1,0:T(8,128)} %reduce-scatter.2.cloned.1.call-done, f32[16,2048]{1,0:T(8,128)S(1)} %copy-done.5, s32[]{:T(128)S(6)} %select_n.8, f32[16]{0:T(128)S(1)} %fusion.12), kind=kOutput, calls=%fused_computation.15 | convolution fusion | flops 37814272 | bytes 569412 | tf_op jit(solution)/shard_map/dot_general | solution.py:126
  (42 shorter events, 0.3 us)
Async XLA Ops:
  6.5 92.0 %copy-start = (bf16[1,256,2048]{2,1,0:T(8,128)(2,1)S(1)}, bf16[1,256,2048]{2,1,0:T(8,128)(2,1)}, u32[]{:S(2)}) copy-start(bf16[1,256,2048]{2,1,0:T(8,128)(2,1)} %param.37) | copy-start | bytes 3145732
  6.5 5.9 %copy-start.1 = (bf16[16,2048]{1,0:T(8,128)(2,1)S(1)}, bf16[16,2048]{1,0:T(8,128)(2,1)}, u32[]{:S(2)}) copy-start(bf16[16,2048]{1,0:T(8,128)(2,1)} %param.20) | copy-start | bytes 196612
  6.5 5.9 %copy-start.6 = (f32[2048]{0:T(1024)S(1)}, f32[2048]{0:T(1024)}, u32[]{:S(2)}) copy-start(f32[2048]{0:T(1024)} %param.23) | copy-start | bytes 24580
  6.5 7.9 %copy-start.2 = (f32[16,2,128,128]{3,2,1,0:T(8,128)S(1)}, f32[16,2,128,128]{3,2,1,0:T(8,128)}, u32[]{:S(2)}) copy-start(f32[16,2,128,128]{3,2,1,0:T(8,128)} %param.22) | copy-start | bytes 6291460
  12.4 4.9 %copy-start.7 = (s32[16,6]{0,1:T(8,128)S(1)}, s32[16,6]{0,1:T(8,128)}, u32[]{:S(2)}) copy-start(s32[16,6]{0,1:T(8,128)} %param.33) | copy-start | bytes 1156
  14.5 11.3 %copy-start.9 = (f32[2048]{0:T(1024)S(1)}, f32[2048]{0:T(1024)}, u32[]{:S(2)}) copy-start(f32[2048]{0:T(1024)} %param.28) | copy-start | bytes 24580
  18.9 41.5 %copy-start.11 = (bf16[1024,256]{1,0:T(8,128)(2,1)S(1)}, bf16[1024,256]{1,0:T(8,128)(2,1)}, u32[]{:S(2)}) copy-start(bf16[1024,256]{1,0:T(8,128)(2,1)} %param.31) | copy-start | bytes 1572868
  27.0 59.8 %all-to-all-start = ((bf16[16,12,1024]{2,1,0:T(8,128)(2,1)}), bf16[16,12,1024]{2,1,0:T(8,128)(2,1)S(1)}, u32[]{:S(2)}, u32[]{:S(2)}) async-start(bf16[16,12,1024]{2,1,0:T(8,128)(2,1)} %reshape.155), calls=%async_computation | async-start | bytes 1048576 | tf_op jit(solution)/shard_map/all_to_all | solution.py:107
  33.5 52.0 %copy-start.4 = (bf16[256,1024]{1,0:T(8,128)(2,1)S(1)}, bf16[256,1024]{1,0:T(8,128)(2,1)}, u32[]{:S(2)}) copy-start(bf16[256,1024]{1,0:T(8,128)(2,1)} %param.32) | copy-start | bytes 1572868
  33.5 51.0 %all-reduce.2.cloned.1.call-start = ((), (), s32[]{:S(2)}) async-start(), calls=%async_computation.4 | async-start | bytes 524288 | tf_op jit(solution)/shard_map/psum | solution.py:138
  62.6 85.8 %reduce-scatter.2.cloned.1.call-start = ((), (), s32[]{:S(2)}) async-start(), calls=%async_computation.5 | async-start | bytes 1114112 | tf_op jit(solution)/shard_map/reduce_scatter | solution.py:144
  85.5 12.6 %copy-start.3 = (bf16[1,2048,256]{2,1,0:T(8,128)(2,1)S(1)}, bf16[1,2048,256]{2,1,0:T(8,128)(2,1)}, u32[]{:S(2)}) copy-start(bf16[1,2048,256]{2,1,0:T(8,128)(2,1)} %param.35) | copy-start | bytes 3145732
  100.9 19.0 %copy-start.10 = (bf16[2048]{0:T(1024)(128)(2,1)S(1)}, bf16[2048]{0:T(1024)(128)(2,1)}, u32[]{:S(2)}) copy-start(bf16[2048]{0:T(1024)(128)(2,1)} %param.29) | copy-start | bytes 12292
  100.9 19.0 %copy-start.8 = (f32[16,6]{0,1:T(8,128)S(1)}, f32[16,6]{0,1:T(8,128)}, u32[]{:S(2)}) copy-start(f32[16,6]{0,1:T(8,128)} %param.34) | copy-start | bytes 1156
  113.0 35.5 %copy-start.5 = (f32[16,2048]{1,0:T(8,128)S(1)}, f32[16,2048]{1,0:T(8,128)}, u32[]{:S(2)}) copy-start(f32[16,2048]{1,0:T(8,128)} %get-tuple-element.6) | copy-start | bytes 393220
  114.2 21.1 %all-to-all-start.2 = ((bf16[16,12,1024]{2,1,0:T(8,128)(2,1)}), bf16[16,12,1024]{2,1,0:T(8,128)(2,1)S(1)}, u32[]{:S(2)}, u32[]{:S(2)}) async-start(bf16[16,12,1024]{2,1,0:T(8,128)(2,1)} %copy.64), calls=%async_computation.2 | async-start | bytes 1048576 | tf_op jit(solution)/shard_map/all_to_all | solution.py:125
Sparse Core Ops, SparseCore 0:
  62.8 21.6 all-reduce.1
  88.1 60.3 reduce-scatter.1
